TPU v7x, 32 devices: a whole 2x2x4 slice. The times are simulated.
32 devices in a mesh: sp: 16 (over z, y, x), tp: 2 (over core).
Axes of the slice: x: 2, y: 2, z: 4, core: 2. Of those that a mesh axis runs over, the one named last changes fastest.
Arguments:
- tokens: bfloat16 [4096, 2048], P('sp'), as said below
- in_gain: float32 [2048], replicated, may hold values from 0.1 to 1.9
- w_query: bfloat16 [2048, 1024], P(None, 'tp'), as said below
- w_key: bfloat16 [2048, 1024], P(None, 'tp'), may hold values from -0.125 to 0.125
- w_value: bfloat16 [2048, 1024], P(None, 'tp'), may hold values from -0.125 to 0.125
- lam: float32 [8], P('tp'), may hold values from 0.3 to 0.8
- sub_gain: float32 [128], replicated, may hold values from 0.1 to 1.9
- w_out: bfloat16 [1024, 2048], P('tp'), may hold values from -0.1875 to 0.1875
Outputs:
- mixed: bfloat16 [4096, 2048], P('sp')
Inputs may be any that keep to these rules, and one draw needn't show every extreme that they name: tokens: normal entries plus, for each block of 64 tokens, a factor times one direction common to all tokens. w_query: independent normal entries.
All inputs are finite; a program needn't handle non-finite values.
Results may differ from a plain program's by a relative error of at most 0.025.
The roundings to bfloat16 on the way count: a program that leaves them out, or rounds other values in their place, can miss the bound.
Values may be sent and summed in bfloat16 or wider, within the bound.
No kernel may reach another device: no remote copies, remote signals or barrier semaphores. Data moves between devices by JAX's collectives and lax.ppermute only.
A program may use at most 64 MiB of HBM per device.

v0:
```python
import jax
import jax.numpy as jnp
from jax import lax
from jax.sharding import PartitionSpec as P

KD = 64
VD = 128


def rotate(vectors, position):
    half = vectors.shape[-1] // 2
    freq = 500000.0 ** (-jnp.arange(0, 2 * half, 2, dtype=jnp.float32) / (2 * half))
    angle = position.astype(jnp.float32)[:, None] * freq[None, :]
    cosine = jnp.cos(angle)[:, None, :]
    sine = jnp.sin(angle)[:, None, :]
    first = vectors[..., :half]
    second = vectors[..., half:]
    return jnp.concatenate(
        [first * cosine - second * sine, second * cosine + first * sine], axis=-1
    )


def shards(tokens, in_gain, w_query, w_key, w_value, lam, sub_gain, w_out):
    span = tokens.shape[0]
    local_heads = lam.shape[0]
    xfloat = tokens.astype(jnp.float32)
    normed = (
        xfloat * lax.rsqrt(jnp.mean(xfloat * xfloat, axis=-1, keepdims=True) + 1e-06) * in_gain
    ).astype(jnp.bfloat16)
    weights_all = jnp.concatenate([w_query, w_key, w_value], axis=1)
    projected = jnp.dot(normed, weights_all, preferred_element_type=jnp.float32)
    qcols = local_heads * 2 * KD
    position = lax.axis_index("sp") * span + jnp.arange(span, dtype=jnp.int32)
    queries = rotate(projected[:, :qcols].reshape(span, 2 * local_heads, KD), position).astype(
        jnp.bfloat16
    )
    queries = queries.reshape(span, local_heads, 2, KD)
    keys = rotate(
        projected[:, qcols : 2 * qcols].reshape(span, 2 * local_heads, KD), position
    ).astype(jnp.bfloat16)
    keys = keys.reshape(span, qcols)
    values = projected[:, 2 * qcols :].astype(jnp.bfloat16)
    scale = KD ** (-0.5)

    def update(carry, key_piece, value_piece):
        top, mass, accum = carry
        count = key_piece.shape[0]
        key_four = key_piece.reshape(count, local_heads, 2, KD)
        value_three = value_piece.reshape(count, local_heads, VD)
        scores = (
            jnp.einsum("qhcd,khcd->hcqk", queries, key_four, preferred_element_type=jnp.float32)
            * scale
        )
        new_top = jnp.maximum(top, jnp.max(scores, axis=-1))
        factor = jnp.exp(top - new_top)
        expo = jnp.exp(scores - new_top[..., None])
        mass = mass * factor + jnp.sum(expo, axis=-1)
        weights = expo.astype(jnp.bfloat16)
        accum = accum * factor[..., None] + jnp.einsum(
            "hcqk,khe->hcqe", weights, value_three, preferred_element_type=jnp.float32
        )
        return (new_top, mass, accum)

    start_carry = (
        jnp.full((local_heads, 2, span), -1e30, jnp.float32),
        jnp.zeros((local_heads, 2, span), jnp.float32),
        jnp.zeros((local_heads, 2, span, VD), jnp.float32),
    )
    carry = start_carry
    key_piece = lax.all_gather(keys, "sp", axis=0, tiled=True)
    value_piece = lax.all_gather(values, "sp", axis=0, tiled=True)
    count = key_piece.shape[0]

    def step_block(inner, items):
        return (update(inner, items[0], items[1]), None)

    blocks = (
        key_piece.reshape(count // 512, 512, key_piece.shape[1]),
        value_piece.reshape(count // 512, 512, value_piece.shape[1]),
    )
    carry, unused = lax.scan(step_block, carry, blocks)
    top, mass, accum = carry
    read = accum / mass[..., None]
    diff = read[:, 0] - lam[:, None, None] * read[:, 1]
    normal = diff * lax.rsqrt(jnp.mean(diff * diff, axis=-1, keepdims=True) + 1e-05) * sub_gain
    attended = jnp.transpose(normal, (1, 0, 2)).reshape(span, local_heads * VD).astype(jnp.bfloat16)
    share = lax.psum_scatter(
        jnp.dot(attended, w_out, preferred_element_type=jnp.float32).astype(jnp.bfloat16),
        "tp",
        scatter_dimension=0,
        tiled=True,
    )
    result = lax.all_gather(share, "tp", axis=0, tiled=True)
    return result


def solution(mesh):
    in_specs = (
        P("sp", None),
        P(),
        P(None, "tp"),
        P(None, "tp"),
        P(None, "tp"),
        P("tp"),
        P(),
        P("tp", None),
    )
    out_specs = P("sp", None)
    return jax.shard_map(shards, mesh=mesh, in_specs=in_specs, out_specs=out_specs, check_vma=False)
```

profile of v0, /device:TPU:0, one launch (start us, length us, event | category | flops | bytes accessed | tf_op | source)
XLA Modules:
  0.0 281.3 jit_solution(3731221670889648921)
XLA Ops:
  6.6 1.7 fusion.19
  8.2 5.0 %fusion.13 = f32[256,1536]{1,0:T(8,128)S(1)} fusion(bf16[2048,512]{1,0:T(8,128)(2,1)} %param.14, bf16[2048,512]{1,0:T(8,128)(2,1)} %param.13, bf16[2048,512]{1,0:T(8,128)(2,1)} %param.12, bf16[256,2048]{1,0:T(8,128)(2,1)} %param.10, f32[2048]{0:T(1024)} %param.11, f32[256]{0:T(256)S(1)} %add_rsqrt_fusion.1), kind=kOutput, calls=%fused_computation.18 | convolution fusion | flops 1631584256 | bytes 8922112 | tf_op jit(solution)/shard_map/dot_general | solution.py:31
  17.2 1.8 slice.71
  19.2 87.7 %all-gather.4.cloned.1.call-done = bf16[4096,512]{0,1:T(8,128)(2,1)} async-done(((bf16[256,512]{0,1:T(8,128)(2,1)}), bf16[4096,512]{0,1:T(8,128)(2,1)}) %all-gather.4.cloned.1.call-update) | async-done | bytes 4194320 | tf_op jit(solution)/shard_map/all_gather | solution.py:70
  106.8 6.5 %copy.16 = bf16[4096,512]{1,0:T(8,128)(2,1)} copy(bf16[4096,512]{0,1:T(8,128)(2,1)} %all-gather.4.cloned.1.call-done) | data formatting | bytes 8388608 | tf_op jit(solution)/shard_map/all_gather | solution.py:70
  113.3 70.1 %all-gather.6.cloned.1.call-done = bf16[4096,512]{1,0:T(8,128)(2,1)} async-done(((bf16[256,512]{1,0:T(8,128)(2,1)}), bf16[4096,512]{1,0:T(8,128)(2,1)}) %all-gather.6.cloned.1.call-update) | async-done | bytes 4194320 | tf_op jit(solution)/shard_map/all_gather | solution.py:71
  183.4 66.4 %while.15 = (s32[]{:T(128)}, f32[4,2,256]{2,1,0:T(2,128)S(1)}, f32[4,2,256]{2,1,0:T(2,128)S(1)}, f32[4,2,256,128]{3,2,1,0:T(8,128)}, bf16[8,512,512]{2,1,0:T(8,1...) while((s32[]{:T(128)}, f32[4,2,256]{2,1,0:T(2,128)S(1)}, ...), condition=%wide.region_4.5_spmd.clone, body=%wide.region_1.4_spmd.clone.sunk | while | flops 411838464 | bytes 30802120 | solution.py:81
  183.4 2.1 constant_dynamic-slice_fusion.3
  185.5 1.3 copy.30
  189.4 1.4 fusion.49
  191.7 2.1 constant_dynamic-slice_fusion.3
  193.8 1.3 copy.30
  197.7 1.4 fusion.49
  200.0 2.1 constant_dynamic-slice_fusion.3
  202.1 1.3 copy.30
  206.0 1.4 fusion.49
  208.3 2.1 constant_dynamic-slice_fusion.3
  214.3 1.4 fusion.49
  216.6 2.1 constant_dynamic-slice_fusion.3
  218.7 1.3 copy.30
  222.6 1.4 fusion.49
  224.9 2.1 constant_dynamic-slice_fusion.3
  230.9 1.4 fusion.49
  233.3 2.1 constant_dynamic-slice_fusion.3
  239.2 1.4 fusion.49
  241.6 2.1 constant_dynamic-slice_fusion.3
  247.5 1.4 fusion.49
  249.9 1.6 copy.21
  251.9 1.7 convolution_convert_fusion
  253.7 7.1 %reduce-scatter.2.cloned.1.call-done = bf16[128,2048]{1,0:T(8,128)(2,1)} async-done(((bf16[256,2048]{1,0:T(8,128)(2,1)}), bf16[128,2048]{1,0:T(8,128)(2,1)}) %reduce-scatter.2.cloned.1.call-update) | async-done | bytes 524304 | tf_op jit(solution)/shard_map/reduce_scatter | solution.py:87
  260.8 11.7 %all-gather.8.cloned.1.call-done = bf16[256,2048]{1,0:T(8,128)(2,1)} async-done(((bf16[128,2048]{1,0:T(8,128)(2,1)}), bf16[256,2048]{1,0:T(8,128)(2,1)}) %all-gather.8.cloned.1.call-update) | async-done | bytes 1048592 | tf_op jit(solution)/shard_map/all_gather | solution.py:93
  272.5 2.3 copy.45
  (134 shorter events, 37.6 us)
Async XLA Ops:
  6.5 245.4 %copy-start = (bf16[512,2048]{1,0:T(8,128)(2,1)S(1)}, bf16[512,2048]{1,0:T(8,128)(2,1)}, u32[]{:S(2)}) copy-start(bf16[512,2048]{1,0:T(8,128)(2,1)} %param.17) | copy-start | bytes 6291460
  6.5 100.3 %all-gather.4.cloned.1.call-start = ((), (), s32[]{:S(2)}) async-start(), calls=%async_computation.1 | async-start | bytes 4456448 | tf_op jit(solution)/shard_map/all_gather | solution.py:70
  13.3 1.4 copy-start.4
  17.2 166.2 %all-gather.6.cloned.1.call-start = ((), (), s32[]{:S(2)}) async-start(), calls=%async_computation.2 | async-start | bytes 4456448 | tf_op jit(solution)/shard_map/all_gather | solution.py:71
  19.1 241.7 %reduce-scatter.2.cloned.1.call-start = ((), (), s32[]{:S(2)}) async-start(), calls=%async_computation.3 | async-start | bytes 1572864 | tf_op jit(solution)/shard_map/reduce_scatter | solution.py:87
  187.8 1.5 copy-start.1
  187.8 1.5 copy-start.2
  190.8 1.0 copy-start.3
  196.1 1.5 copy-start.1
  196.1 1.5 copy-start.2
  199.1 1.0 copy-start.3
  204.4 1.5 copy-start.1
  204.4 1.5 copy-start.2
  207.4 1.0 copy-start.3
  212.7 1.5 copy-start.1
  212.7 1.5 copy-start.2
  215.7 1.0 copy-start.3
  221.0 1.5 copy-start.1
  221.0 1.5 copy-start.2
  224.0 1.0 copy-start.3
  229.3 1.5 copy-start.1
  229.3 1.5 copy-start.2
  232.3 1.0 copy-start.3
  237.6 1.5 copy-start.1
  237.6 1.5 copy-start.2
  240.6 1.0 copy-start.3
  245.9 1.5 copy-start.1
  245.9 1.5 copy-start.2
  248.9 1.0 copy-start.3
  249.9 1.7 copy-start.5
  249.9 1.9 copy-start.6
  253.6 18.8 %all-gather.8.cloned.1.call-start = ((), (), s32[]{:S(2)}) async-start(), calls=%async_computation.4 | async-start | bytes 1572864 | tf_op jit(solution)/shard_map/all_gather | solution.py:93
Sparse Core Ops, SparseCore 0:
  17.3 89.4 all-gather.3
  109.6 73.7 all-gather.5
  253.8 6.9 reduce-scatter.1
  262.2 10.2 all-gather.7
where the time goes:
time: 282 us; the launch traced here: 281 us
  waiting for transfers between devices  177 us (63%)
  local copies, waits for them, and re-layouts  57.7 us (20%)
  matrix products  24.1 us (9%)
  between operations  13.3 us (5%)
  other arithmetic  9.1 us (3%)
    all_gather x1, waiting for transfers between devices, shards(): key_piece = lax.all_gather(keys, 'sp', axis=0, tiled=True)  87.7 us
    all_gather x1, waiting for transfers between devices, shards(): value_piece = lax.all_gather(values, 'sp', axis=0, tiled=True)  70.1 us
    dynamic_slice x24, local copies, waits for them, and re-layouts, shards(): carry, unused = lax.scan(step_block, carry, blocks)  35 us
    all_gather x1, waiting for transfers between devices, shards(): result = lax.all_gather(share, 'tp', axis=0, tiled=True)  11.7 us
    dot_general x8, matrix products, update(): jnp.einsum('hcqk,khe->hcqe', weights, value_three, preferred_element_type...  11.1 us
    while x56, local copies, waits for them, and re-layouts  7.71 us
    reduce_scatter x1, waiting for transfers between devices, shards(): lax.psum_scatter(jnp.dot(attended, w_out, preferred_element_type=jnp.floa...  7.07 us
    all_gather x1, local copies, waits for them, and re-layouts, shards(): key_piece = lax.all_gather(keys, 'sp', axis=0, tiled=True)  6.49 us
  transfers between devices with their start and end apart: 4, of which 4 were waited for; matrix products, arithmetic and copies ran while one was open for 3% of the time, Pallas kernels for 0%

commit v1 on v0

--- a/solution.py
+++ b/solution.py
@@ -68,7 +68,8 @@
     )
     carry = start_carry
     key_piece = lax.all_gather(keys, "sp", axis=0, tiled=True)
-    value_piece = lax.all_gather(values, "sp", axis=0, tiled=True)
+    sent = jnp.stack([values] * lax.axis_size("sp"))
+    value_piece = jnp.concatenate(lax.all_to_all(sent, "sp", 0, 0), axis=0)
     count = key_piece.shape[0]
 
     def step_block(inner, items):

time: 282 us -> 279 us (0.989)
  waiting for transfers between devices: 177 us -> 163 us
  starting transfers between devices: 0.13 us -> 8.61 us
    all_gather x1 -> x0, waiting for transfers between devices: 70.1 us -> none  [shards(): value_piece = lax.all_gather(values, 'sp', axis=0, tiled=True)]
    all_gather x1, waiting for transfers between devices: 87.7 us -> 140 us  [shards(): key_piece = lax.all_gather(keys, 'sp', axis=0, tiled=True)]
    all_to_all x0 -> x1, starting transfers between devices: none -> 8.53 us  [shards(): value_piece = jnp.concatenate(lax.all_to_all(sent, 'sp', 0, 0), axis=0)]
    reduce_scatter x1, waiting for transfers between devices: 7.07 us -> 10.4 us  [shards(): lax.psum_scatter(jnp.dot(attended, w_out, preferred_element_type=jnp.floa...]
  transfers between devices with their start and end apart: 4 -> 4, of which waited for: 4 -> 3; matrix products, arithmetic and copies ran while one was open for 3% -> 4% of each run, Pallas kernels for 0% -> 0%
where the time goes in v1:
time: 279 us; the launch traced here: 278 us
  waiting for transfers between devices  163 us (58%)
  local copies, waits for them, and re-layouts  59.3 us (21%)
  matrix products  24.1 us (9%)
  between operations  13.3 us (5%)
  other arithmetic  9.75 us (3%)
  starting transfers between devices  8.61 us (3%)
    all_gather x1, waiting for transfers between devices, shards(): key_piece = lax.all_gather(keys, 'sp', axis=0, tiled=True)  140 us
    dynamic_slice x24, local copies, waits for them, and re-layouts, shards(): carry, unused = lax.scan(step_block, carry, blocks)  35 us
    all_gather x1, waiting for transfers between devices, shards(): result = lax.all_gather(share, 'tp', axis=0, tiled=True)  11.8 us
    dot_general x8, matrix products, update(): jnp.einsum('hcqk,khe->hcqe', weights, value_three, preferred_element_type...  11.1 us
    reduce_scatter x1, waiting for transfers between devices, shards(): lax.psum_scatter(jnp.dot(attended, w_out, preferred_element_type=jnp.floa...  10.4 us
    all_to_all x1, starting transfers between devices, shards(): value_piece = jnp.concatenate(lax.all_to_all(sent, 'sp', 0, 0), axis=0)  8.53 us
    while x56, local copies, waits for them, and re-layouts  7.71 us
    all_gather x1, local copies, waits for them, and re-layouts, shards(): key_piece = lax.all_gather(keys, 'sp', axis=0, tiled=True)  6.49 us
  transfers between devices with their start and end apart: 4, of which 3 were waited for; matrix products, arithmetic and copies ran while one was open for 4% of the time, Pallas kernels for 0%

profile of v1, /device:TPU:0, one launch (start us, length us, event | category | flops | bytes accessed | tf_op | source)
XLA Modules:
  0.0 278.0 jit_solution(15432155339395088410)
XLA Ops:
  6.6 1.7 fusion.19
  8.2 5.0 %fusion.13 = f32[256,1536]{1,0:T(8,128)S(1)} fusion(bf16[2048,512]{1,0:T(8,128)(2,1)} %param.14, bf16[2048,512]{1,0:T(8,128)(2,1)} %param.13, bf16[2048,512]{1,0:T(8,128)(2,1)} %param.12, bf16[256,2048]{1,0:T(8,128)(2,1)} %param.10, f32[2048]{0:T(1024)} %param.11, f32[256]{0:T(256)S(1)} %add_rsqrt_fusion.1), kind=kOutput, calls=%fused_computation.18 | convolution fusion | flops 1631584256 | bytes 8922112 | tf_op jit(solution)/shard_map/dot_general | solution.py:31
  18.9 2.3 stack.2
  21.2 8.5 %all-to-all-start = ((bf16[16,256,512]{2,1,0:T(8,128)(2,1)}), bf16[16,256,512]{2,1,0:T(8,128)(2,1)}, u32[]{:S(2)}, u32[]{:S(2)}) async-start(bf16[16,256,512]{2,1,0:T(8,128)(2,1)} %stack.2), calls=%async_computation | async-start | bytes 8388608 | tf_op jit(solution)/shard_map/all_to_all | solution.py:72
  29.9 140.2 %all-gather.3.cloned.1.call-done = bf16[4096,512]{0,1:T(8,128)(2,1)} async-done(((bf16[256,512]{0,1:T(8,128)(2,1)}), bf16[4096,512]{0,1:T(8,128)(2,1)}) %all-gather.3.cloned.1.call-update) | async-done | bytes 4194320 | tf_op jit(solution)/shard_map/all_gather | solution.py:70
  170.1 6.5 %copy.24 = bf16[4096,512]{1,0:T(8,128)(2,1)} copy(bf16[4096,512]{0,1:T(8,128)(2,1)} %all-gather.3.cloned.1.call-done) | data formatting | bytes 8388608 | tf_op jit(solution)/shard_map/all_gather | solution.py:70
  176.6 66.4 %while.15 = (s32[]{:T(128)}, f32[4,2,256]{2,1,0:T(2,128)S(1)}, f32[4,2,256]{2,1,0:T(2,128)S(1)}, f32[4,2,256,128]{3,2,1,0:T(8,128)}, bf16[8,512,512]{2,1,0:T(8,1...) while((s32[]{:T(128)}, f32[4,2,256]{2,1,0:T(2,128)S(1)}, ...), condition=%wide.region_4.5_spmd.clone, body=%wide.region_1.4_spmd.clone.sunk | while | flops 411838464 | bytes 30802120 | solution.py:82
  176.6 2.1 constant_dynamic-slice_fusion.3
  178.7 1.3 copy.38
  182.6 1.4 fusion.49
  184.9 2.1 constant_dynamic-slice_fusion.3
  187.0 1.3 copy.38
  190.9 1.4 fusion.49
  193.2 2.1 constant_dynamic-slice_fusion.3
  199.2 1.4 fusion.49
  201.5 2.1 constant_dynamic-slice_fusion.3
  203.6 1.3 copy.38
  207.5 1.4 fusion.49
  209.8 2.1 constant_dynamic-slice_fusion.3
  215.8 1.4 fusion.49
  218.1 2.1 constant_dynamic-slice_fusion.3
  224.1 1.4 fusion.49
  226.4 2.1 constant_dynamic-slice_fusion.3
  232.4 1.4 fusion.49
  234.8 2.1 constant_dynamic-slice_fusion.3
  236.8 1.3 copy.38
  240.7 1.4 fusion.49
  243.1 1.6 copy.29
  245.1 1.7 convolution_convert_fusion
  246.9 10.4 %reduce-scatter.2.cloned.1.call-done = bf16[128,2048]{1,0:T(8,128)(2,1)} async-done(((bf16[256,2048]{1,0:T(8,128)(2,1)}), bf16[128,2048]{1,0:T(8,128)(2,1)}) %reduce-scatter.2.cloned.1.call-update) | async-done | bytes 524304 | tf_op jit(solution)/shard_map/reduce_scatter | solution.py:88
  257.3 11.8 %all-gather.5.cloned.1.call-done = bf16[256,2048]{1,0:T(8,128)(2,1)} async-done(((bf16[128,2048]{1,0:T(8,128)(2,1)}), bf16[256,2048]{1,0:T(8,128)(2,1)}) %all-gather.5.cloned.1.call-update) | async-done | bytes 1048592 | tf_op jit(solution)/shard_map/all_gather | solution.py:94
  269.2 2.3 copy.53
  (136 shorter events, 39.3 us)
Async XLA Ops:
  6.5 238.6 %copy-start = (bf16[512,2048]{1,0:T(8,128)(2,1)S(1)}, bf16[512,2048]{1,0:T(8,128)(2,1)}, u32[]{:S(2)}) copy-start(bf16[512,2048]{1,0:T(8,128)(2,1)} %param.17) | copy-start | bytes 6291460
  6.5 163.6 %all-gather.3.cloned.1.call-start = ((), (), s32[]{:S(2)}) async-start(), calls=%async_computation.2 | async-start | bytes 4456448 | tf_op jit(solution)/shard_map/all_gather | solution.py:70
  13.3 1.4 copy-start.4
  21.2 8.6 %copy-start.5 = (bf16[256,8,32]{0,2,1:T(8,128)(2,1)S(1)}, bf16[256,8,32]{0,2,1:T(8,128)(2,1)}, u32[]{:S(2)}) copy-start(bf16[256,8,32]{0,2,1:T(8,128)(2,1)} %get-tuple-element.106) | copy-start | bytes 393220
  21.2 155.4 %all-to-all-start = ((bf16[16,256,512]{2,1,0:T(8,128)(2,1)}), bf16[16,256,512]{2,1,0:T(8,128)(2,1)}, u32[]{:S(2)}, u32[]{:S(2)}) async-start(bf16[16,256,512]{2,1,0:T(8,128)(2,1)} %stack.2), calls=%async_computation | async-start | bytes 8388608 | tf_op jit(solution)/shard_map/all_to_all | solution.py:72
  29.8 227.5 %reduce-scatter.2.cloned.1.call-start = ((), (), s32[]{:S(2)}) async-start(), calls=%async_computation.3 | async-start | bytes 1572864 | tf_op jit(solution)/shard_map/reduce_scatter | solution.py:88
  181.0 1.5 copy-start.1
  181.0 1.6 copy-start.2
  184.0 1.0 copy-start.3
  189.3 1.5 copy-start.1
  189.3 1.6 copy-start.2
  192.3 1.0 copy-start.3
  197.6 1.5 copy-start.1
  197.6 1.5 copy-start.2
  200.6 1.0 copy-start.3
  205.9 1.5 copy-start.1
  205.9 1.5 copy-start.2
  208.9 1.0 copy-start.3
  214.2 1.5 copy-start.1
  214.2 1.5 copy-start.2
  217.2 1.0 copy-start.3
  222.5 1.5 copy-start.1
  222.5 1.5 copy-start.2
  225.5 1.0 copy-start.3
  230.8 1.5 copy-start.1
  230.8 1.5 copy-start.2
  239.1 1.5 copy-start.1
  239.1 1.5 copy-start.2
  242.1 1.0 copy-start.3
  243.1 1.7 copy-start.6
  243.1 1.9 copy-start.7
  246.8 22.3 %all-gather.5.cloned.1.call-start = ((), (), s32[]{:S(2)}) async-start(), calls=%async_computation.4 | async-start | bytes 1572864 | tf_op jit(solution)/shard_map/all_gather | solution.py:94
  (1 other events, 1.0 us)
Sparse Core Ops, SparseCore 0:
  18.0 152.1 all-gather.2
  247.0 10.3 reduce-scatter.1
  258.9 10.2 all-gather.4
